TPU v7x, 32 devices: a whole 2x2x4 slice. The times are simulated.
32 devices in a mesh: dp: 4 (over y, x), kv: 4 (over z), tp: 2 (over core).
Axes of the slice: x: 2, y: 2, z: 4, core: 2. Of those that a mesh axis runs over, the one named last changes fastest.
Arguments:
- tokens: bfloat16 [32, 4096], P('dp', 'kv'), parts along dimension 0, may hold values from -16 to 16
- gain_mix: float32 [4096], P('kv'), may hold values from 0.1 to 1.9
- w_query: bfloat16 [4096, 2048], P('kv', 'tp'), may hold values from -0.09375 to 0.09375
- w_key: bfloat16 [4096, 2048], P('kv', 'tp'), may hold values from -0.09375 to 0.09375
- w_value: bfloat16 [4096, 2048], P('kv', 'tp'), may hold values from -0.09375 to 0.09375
- w_igate: bfloat16 [4096, 16], P('kv', 'tp'), may hold values from -0.09375 to 0.09375
- w_fgate: bfloat16 [4096, 16], P('kv', 'tp'), may hold values from -0.09375 to 0.09375
- bias_igate: float32 [16], P('tp'), may hold values from -1 to 1
- bias_fgate: float32 [16], P('tp'), may hold values from -1 to 4
- memory: float32 [32, 16, 128, 128], P(('dp', 'kv'), 'tp'), parts along dimension 0, may hold values from -0.8 to 0.8
- normalizer: float32 [32, 16, 128], P(('dp', 'kv'), 'tp'), parts along dimension 0, may hold values from -0.8 to 0.8
- stabilizer: float32 [32, 16], P(('dp', 'kv'), 'tp'), parts along dimension 0, may hold values from -1.5 to 1.5
- w_output: bfloat16 [2048, 4096], P('tp', 'kv'), may hold values from -0.125 to 0.125
- gain_mlp: float32 [4096], replicated, may hold values from 0.1 to 1.9
- w_gate: bfloat16 [4096, 11264], P(None, ('kv', 'tp')), may hold values from -0.09375 to 0.09375
- w_up: bfloat16 [4096, 11264], P(None, ('kv', 'tp')), may hold values from -0.09375 to 0.09375
- w_down: bfloat16 [11264, 4096], P(('kv', 'tp')), may hold values from -0.078125 to 0.078125
Outputs:
- mixed: bfloat16 [32, 4096], P('dp', ('kv', 'tp')), parts along dimension 0
- memory_next: float32 [32, 16, 128, 128], P(('dp', 'kv'), 'tp'), parts along dimension 0
- normalizer_next: float32 [32, 16, 128], P(('dp', 'kv'), 'tp'), parts along dimension 0
- stabilizer_next: float32 [32, 16], P(('dp', 'kv'), 'tp'), parts along dimension 0
There are 4 independent parts, one for each index of `dp`. A program takes and returns all parts, laid end to end along the dimension named above; an argument that names none is the same for every part. Nothing has to cross between parts.
All inputs are finite; a program needn't handle non-finite values.
Results may differ from a plain program's by a relative error of at most 0.014.
Values may be sent and summed in bfloat16 or wider, within the bound.
A program may use at most 128 MiB of HBM per device.

v0:
```python
import jax
import jax.numpy as jnp
from jax import lax
from jax.sharding import PartitionSpec as P

D = 4096


epsilon = 1e-06


def cell_update(
    queries, key_proj, values, in_gate, log_forget, memory, normalizer, stabilizer, head_count
):
    batch_rows = queries.shape[0]
    query_heads = queries.astype(jnp.float32).reshape(batch_rows, head_count, -1)
    head_dim = query_heads.shape[2]
    key_heads = key_proj.astype(jnp.float32).reshape(
        batch_rows, head_count, head_dim
    ) * head_dim ** (-0.5)
    value_heads = values.astype(jnp.float32).reshape(batch_rows, head_count, head_dim)
    stab_next = jnp.maximum(stabilizer + log_forget, in_gate)
    keeping = jnp.exp(stabilizer + log_forget - stab_next)
    fresh_weight = jnp.exp(in_gate - stab_next)
    memory_next = (
        keeping[:, :, None, None] * memory
        + fresh_weight[:, :, None, None] * value_heads[:, :, :, None] * key_heads[:, :, None, :]
    )
    norm_next = keeping[:, :, None] * normalizer + fresh_weight[:, :, None] * key_heads
    numerator = jnp.einsum(
        "bhvk,bhk->bhv", memory_next, query_heads, precision=lax.Precision.HIGHEST
    )
    denominator = jnp.einsum("bhk,bhk->bh", norm_next, query_heads, precision=lax.Precision.HIGHEST)
    denominator = jnp.maximum(jnp.abs(denominator), jnp.exp(-stab_next))
    hidden = (numerator / denominator[:, :, None]).reshape(batch_rows, -1).astype(jnp.bfloat16)
    return (hidden, memory_next, norm_next, stab_next)


def mixer_block(residual, gain_mlp, w_gate, w_up, w_down):
    full_rows = lax.all_gather(residual, "kv", axis=1, tiled=True).astype(jnp.float32)
    scaling = lax.rsqrt(jnp.mean(full_rows * full_rows, axis=1, keepdims=True) + epsilon)
    normed = (full_rows * scaling * gain_mlp).astype(jnp.bfloat16)
    gate_act = jnp.dot(normed, w_gate, preferred_element_type=jnp.float32)
    up_act = jnp.dot(normed, w_up, preferred_element_type=jnp.float32)
    activated = (jax.nn.silu(gate_act) * up_act).astype(jnp.bfloat16)
    down_terms = jnp.dot(activated, w_down, preferred_element_type=jnp.float32)
    return lax.psum_scatter(down_terms, ("kv", "tp"), scatter_dimension=1, tiled=True)


def local(
    tokens,
    gain_mix,
    w_query,
    w_key,
    w_value,
    w_igate,
    w_fgate,
    bias_igate,
    bias_fgate,
    memory,
    normalizer,
    stabilizer,
    w_output,
    gain_mlp,
    w_gate,
    w_up,
    w_down,
):
    tok_float = tokens.astype(jnp.float32)
    scaled = (tok_float * gain_mix).astype(jnp.bfloat16)
    part_squares = jnp.sum(tok_float * tok_float, axis=1)
    query_part = jnp.dot(scaled, w_query, preferred_element_type=jnp.float32)
    key_part = jnp.dot(scaled, w_key, preferred_element_type=jnp.float32)
    value_part = jnp.dot(scaled, w_value, preferred_element_type=jnp.float32)
    igate_part = jnp.dot(scaled, w_igate, preferred_element_type=jnp.float32)
    fgate_part = jnp.dot(scaled, w_fgate, preferred_element_type=jnp.float32)
    query_sum, key_sum, value_sum, igate_sum, fgate_sum, own_squares = (
        lax.psum_scatter(query_part, "kv", scatter_dimension=0, tiled=True),
        lax.psum_scatter(key_part, "kv", scatter_dimension=0, tiled=True),
        lax.psum_scatter(value_part, "kv", scatter_dimension=0, tiled=True),
        lax.psum_scatter(igate_part, "kv", scatter_dimension=0, tiled=True),
        lax.psum_scatter(fgate_part, "kv", scatter_dimension=0, tiled=True),
        lax.psum_scatter(part_squares, "kv", scatter_dimension=0, tiled=True),
    )
    scaling = lax.rsqrt(own_squares / D + epsilon)[:, None]
    queries = (scaling * query_sum).astype(jnp.bfloat16)
    key_proj = (scaling * key_sum).astype(jnp.bfloat16)
    values = (scaling * value_sum).astype(jnp.bfloat16)
    in_gate = scaling * igate_sum + bias_igate
    log_forget = jax.nn.log_sigmoid(scaling * fgate_sum + bias_fgate)
    hidden, memory_next, norm_next, stab_next = cell_update(
        queries,
        key_proj,
        values,
        in_gate,
        log_forget,
        memory,
        normalizer,
        stabilizer,
        memory.shape[1],
    )
    branch_part = jnp.dot(
        lax.all_gather(hidden, "kv", axis=0, tiled=True),
        w_output,
        preferred_element_type=jnp.float32,
    )
    branch = lax.psum(branch_part.astype(jnp.bfloat16), "tp").astype(jnp.float32)
    residual = (tok_float + branch).astype(jnp.bfloat16)
    mixed_terms = mixer_block(residual, gain_mlp, w_gate, w_up, w_down)
    columns = mixed_terms.shape[1]
    residual_own = lax.dynamic_slice_in_dim(residual, lax.axis_index("tp") * columns, columns, 1)
    mixed = (residual_own.astype(jnp.float32) + mixed_terms).astype(jnp.bfloat16)
    return (mixed, memory_next, norm_next, stab_next)


def solution(mesh):
    placed = (
        P("dp", "kv"),
        P("kv"),
        P("kv", "tp"),
        P("kv", "tp"),
        P("kv", "tp"),
        P("kv", "tp"),
        P("kv", "tp"),
        P("tp"),
        P("tp"),
        P(("dp", "kv"), "tp", None, None),
        P(("dp", "kv"), "tp", None),
        P(("dp", "kv"), "tp"),
        P("tp", "kv"),
        P(),
        P(None, ("kv", "tp")),
        P(None, ("kv", "tp")),
        P(("kv", "tp"), None),
    )
    return jax.shard_map(
        local,
        mesh=mesh,
        in_specs=placed,
        out_specs=(
            P("dp", ("kv", "tp")),
            P(("dp", "kv"), "tp", None, None),
            P(("dp", "kv"), "tp", None),
            P(("dp", "kv"), "tp"),
        ),
        check_vma=False,
    )
```

profile of v0, /device:TPU:0, one launch (start us, length us, event | category | flops | bytes accessed | tf_op | source)
XLA Modules:
  0.0 146.3 jit_solution(16323589143473186552)
XLA Ops:
  7.2 0.0 copy-start
  7.2 0.0 all-reduce.9.cloned.1.call-start
  7.3 1.5 %fusion.10 = f32[8]{0:T(128)} fusion(bf16[8,1024]{1,0:T(8,128)(2,1)} %param.17), kind=kLoop, calls=%fused_computation.18 | loop fusion | flops 24568 | bytes 16416 | tf_op jit(solution)/shard_map/reduce_sum | solution.py:71
  8.8 0.0 copy-done
  8.8 1.9 %fusion.31 = f32[8,1024]{1,0:T(8,128)} fusion(bf16[1024,1024]{1,0:T(8,128)(2,1)S(1)} %copy-done, bf16[8,1024]{1,0:T(8,128)(2,1)} %param.17, f32[1024]{0:T(1024)} %param.18), kind=kOutput, calls=%fused_computation.56 | convolution fusion | flops 16801792 | bytes 2150400 | tf_op jit(solution)/shard_map/dot_general | solution.py:72
  10.7 0.0 copy-start.14
  10.7 1.0 fusion.33
  11.7 1.0 fusion.35
  12.7 0.7 fusion.37
  13.5 0.7 fusion.39
  14.2 0.0 all-reduce.9.cloned.1.call-update
  14.2 0.0 reduce-scatter.2.cloned.1.call-start
  14.3 0.6 dynamic-slice
  15.5 36.6 %all-reduce.9.cloned.1.call-done = (f32[8,1024]{1,0:T(8,128)}, f32[8]{0:T(128)}, f32[8,1024]{1,0:T(8,128)}, f32[8,8]{1,0:T(8,128)}, f32[8,8]{1,0:T(8,128)}, /*index=5*/f32[8,1024]{1,0:T(8,128)}) async-done(((f32[8,1024]{1,0:T(8,128)}, f32[8]{0:T(128)}, f32[8,1024]{1,0:T(8,128)}, f32[8,8]{1,0:T(8,128)}, f32[8,8]{1,0:T(8,128)}, /*index=5*/f32[8,1024]{1,0:T(8,128)}), (f32[8,1024]{1,0:T(8,128)}, f32[8]{0:T(128)}, ...) | async-done | bytes 98864
  52.1 0.7 fusion.30
  52.7 0.9 fusion.19
  53.6 0.8 broadcast_multiply_fusion
  54.5 0.0 copy-start.9
  54.5 0.7 multiply_reduce_fusion
  55.2 1.6 %multiply_add_fusion = f32[2,8,128,128]{3,2,1,0:T(8,128)S(1)} fusion(f32[2,8,128,128]{3,2,1,0:T(8,128)} %param.26, f32[2,8,128]{2,1,0:T(8,128)S(1)} %get-tuple-element.16, f32[2,8,128]{2,1,0:T(8,128)S(1)} %get-tuple-element.20, f32[2,8]{1,0:T(2,128)S(1)} %subtract_exponential_fusion.1), kind=kLoop, calls=%fused_computation.3 | loop fusion | flops 786432 | bytes 2113600 | tf_op jit(solution)/shard_map/add | solution.py:26
  56.8 0.9 fusion.46
  57.7 0.1 divide_convert_fusion
  57.8 13.3 %all-gather = bf16[4,2,1024]{2,1,0:T(2,128)(2,1)S(1)} all-gather(bf16[1,2,1024]{2,1,0:T(2,128)(2,1)S(1)} %reshape.58), channel_id=1, replica_groups=mesh['dp'=4,'kv'=4,'tp'=2] {'kv'}, dimensions={0}, use_global_device_ids=true | all-gather | bytes 20480 | tf_op jit(solution)/shard_map/all_gather | solution.py:103
  71.1 2.0 %convolution_convert_fusion = bf16[8,1024]{1,0:T(8,128)(2,1)S(1)} fusion(bf16[8,1024]{1,0:T(8,128)(2,1)S(1)} %reshape.59, bf16[1024,1024]{1,0:T(8,128)(2,1)} %param.29), kind=kOutput, calls=%fused_computation.2 | convolution fusion | flops 16785408 | bytes 2129920 | tf_op jit(solution)/shard_map/dot_general | solution.py:102
  73.1 3.4 %psum.7 = bf16[8,1024]{1,0:T(8,128)(2,1)S(1)} all-reduce(bf16[8,1024]{1,0:T(8,128)(2,1)S(1)} %convolution_convert_fusion), channel_id=1, replica_groups=mesh['dp'=4,'kv'=4,'tp'=2] {'tp'}, use_global_device_ids=true, to_apply=%region_7.8 | all-reduce | flops 8192 | bytes 32768 | tf_op jit(solution)/shard_map/psum | solution.py:107
  76.5 13.1 %all_gather.7 = bf16[8,4096]{1,0:T(8,128)(2,1)S(1)} all-gather(bf16[8,1024]{1,0:T(8,128)(2,1)S(1)} %fusion.12), channel_id=1, replica_groups=mesh['dp'=4,'kv'=4,'tp'=2] {'kv'}, dimensions={1}, use_global_device_ids=true | all-gather | bytes 81920 | tf_op jit(solution)/shard_map/all_gather | solution.py:40
  89.6 0.1 fusion.2
  89.8 5.9 %fusion.16 = f32[8,1408]{1,0:T(8,128)S(1)} fusion(bf16[4096,1408]{1,0:T(8,128)(2,1)} %param.31, bf16[8,4096]{1,0:T(8,128)(2,1)S(1)} %all_gather.7, f32[4096]{0:T(1024)S(1)} %copy-done.5, f32[8]{0:T(128)S(1)} %add_rsqrt_fusion), kind=kOutput, calls=%fused_computation.23 | convolution fusion | flops 92405760 | bytes 11661344 | tf_op jit(solution)/shard_map/dot_general | solution.py:43
  95.7 11.7 %fusion.1 = f32[8,4096]{1,0:T(8,128)} fusion(bf16[1408,4096]{1,0:T(8,128)(2,1)} %param.33, bf16[4096,1408]{1,0:T(8,128)(2,1)} %param.32, f32[8,1408]{1,0:T(8,128)S(1)} %fusion.16, bf16[8,4096]{1,0:T(8,128)(2,1)S(1)} %all_gather.7, f32[4096]{0:T(1024)S(1)} %copy-done.5, f32[8]{0:T(128)S(1)} %add_rsqrt_fusion), kind=kOutput, calls=%fused_computation.4 | convolution fusion | flops 184748032 | bytes 23326752 | tf_op jit(solution)/shard_map/dot_general | solution.py:46
  107.4 0.0 reduce-scatter.2.cloned.1.call-update
  107.4 30.8 %reduce-scatter.2.cloned.1.call-done = f32[8,512]{1,0:T(8,128)} async-done(((f32[8,4096]{1,0:T(8,128)}), f32[8,512]{1,0:T(8,128)}) %reduce-scatter.2.cloned.1.call-update) | async-done | bytes 16400 | tf_op jit(solution)/shard_map/reduce_scatter | solution.py:47
  138.2 1.3 add_convert_fusion
  (33 shorter events, 0.2 us)
Async XLA Ops:
  7.2 1.6 %copy-start = (bf16[1024,1024]{1,0:T(8,128)(2,1)S(1)}, bf16[1024,1024]{1,0:T(8,128)(2,1)}, u32[]{:S(2)}) copy-start(bf16[1024,1024]{1,0:T(8,128)(2,1)} %param.19) | copy-start | bytes 6291460
  7.2 3.5 %copy-start.4 = (bf16[8,1024]{1,0:T(8,128)(2,1)S(1)}, bf16[8,1024]{1,0:T(8,128)(2,1)}, u32[]{:S(2)}) copy-start(bf16[8,1024]{1,0:T(8,128)(2,1)} %param.17) | copy-start | bytes 49156
  7.2 3.5 %copy-start.6 = (f32[1024]{0:T(1024)S(1)}, f32[1024]{0:T(1024)}, u32[]{:S(2)}) copy-start(f32[1024]{0:T(1024)} %param.18) | copy-start | bytes 12292
  7.2 44.8 %all-reduce.9.cloned.1.call-start = ((), (), s32[]{:S(2)}) async-start(), calls=%async_computation.2 | async-start | bytes 214016
  7.3 3.4 %copy-start.2 = (bf16[1024,1024]{1,0:T(8,128)(2,1)S(1)}, bf16[1024,1024]{1,0:T(8,128)(2,1)}, u32[]{:S(2)}) copy-start(bf16[1024,1024]{1,0:T(8,128)(2,1)} %param.20) | copy-start | bytes 6291460
  8.8 3.0 %copy-start.3 = (bf16[1024,1024]{1,0:T(8,128)(2,1)S(1)}, bf16[1024,1024]{1,0:T(8,128)(2,1)}, u32[]{:S(2)}) copy-start(bf16[1024,1024]{1,0:T(8,128)(2,1)} %param.21) | copy-start | bytes 6291460
  10.7 2.1 %copy-start.7 = (bf16[1024,8]{0,1:T(8,128)(2,1)S(1)}, bf16[1024,8]{0,1:T(8,128)(2,1)}, u32[]{:S(2)}) copy-start(bf16[1024,8]{0,1:T(8,128)(2,1)} %param.22) | copy-start | bytes 49156
  10.7 2.8 %copy-start.8 = (bf16[1024,8]{0,1:T(8,128)(2,1)S(1)}, bf16[1024,8]{0,1:T(8,128)(2,1)}, u32[]{:S(2)}) copy-start(bf16[1024,8]{0,1:T(8,128)(2,1)} %param.23) | copy-start | bytes 49156
  10.7 3.6 %copy-start.14 = (u32[32]{0:T(128)S(1)}, u32[32]{0:T(128)}, u32[]{:S(2)}) copy-start(u32[32]{0:T(128)} %constant.34) | copy-start | bytes 388
  10.7 42.9 %copy-start.11 = (f32[2,8]{1,0:T(2,128)S(1)}, f32[2,8]{1,0:T(2,128)}, u32[]{:S(2)}) copy-start(f32[2,8]{1,0:T(2,128)} %param.28) | copy-start | bytes 196
  10.7 42.9 %copy-start.12 = (f32[8]{0:T(128)S(1)}, f32[8]{0:T(128)}, u32[]{:S(2)}) copy-start(f32[8]{0:T(128)} %param.24) | copy-start | bytes 100
  10.7 42.9 %copy-start.13 = (f32[8]{0:T(128)S(1)}, f32[8]{0:T(128)}, u32[]{:S(2)}) copy-start(f32[8]{0:T(128)} %param.25) | copy-start | bytes 100
  10.7 43.8 %copy-start.10 = (f32[2,8,128]{2,1,0:T(8,128)S(1)}, f32[2,8,128]{2,1,0:T(8,128)}, u32[]{:S(2)}) copy-start(f32[2,8,128]{2,1,0:T(8,128)} %param.27) | copy-start | bytes 24580
  14.2 124.0 %reduce-scatter.2.cloned.1.call-start = ((), (), s32[]{:S(2)}) async-start(), calls=%async_computation.1 | async-start | bytes 147456 | tf_op jit(solution)/shard_map/reduce_scatter | solution.py:47
  54.5 18.7 %copy-start.9 = (f32[2,8]{1,0:T(2,128)}, f32[2,8]{1,0:T(2,128)S(1)}, u32[]{:S(2)}) copy-start(f32[2,8]{1,0:T(2,128)S(1)} %get-tuple-element.14) | copy-start | bytes 196
  56.8 38.9 %copy-start.1 = (f32[2,8,128,128]{3,2,1,0:T(8,128)}, f32[2,8,128,128]{3,2,1,0:T(8,128)S(1)}, u32[]{:S(2)}) copy-start(f32[2,8,128,128]{3,2,1,0:T(8,128)S(1)} %multiply_add_fusion) | copy-start | bytes 3145732
  56.8 33.0 %copy-start.5 = (f32[4096]{0:T(1024)S(1)}, f32[4096]{0:T(1024)}, u32[]{:S(2)}) copy-start(f32[4096]{0:T(1024)} %param.30) | copy-start | bytes 49156
Sparse Core Ops, SparseCore 0:
  14.3 37.6 all-reduce.8
  107.5 30.6 reduce-scatter.1
where the time goes:
time: 147 us; the launch traced here: 146 us
  waiting for transfers between devices  67.4 us (46%)
  blocking collectives  29.8 us (20%)
  matrix products  25.7 us (17%)
  between operations  14.9 us (10%)
  other arithmetic  7.7 us (5%)
    unnamed x3, waiting for transfers between devices  36.6 us
    reduce_scatter x1, waiting for transfers between devices, mixer_block(): lax.psum_scatter(down_terms, ('kv', 'tp'), scatter_dimension=1, tiled=True)  30.8 us
    all_gather x1, blocking collectives, local(): lax.all_gather(hidden, 'kv', axis=0, tiled=True)  13.3 us
    all_gather x1, blocking collectives, mixer_block(): lax.all_gather(residual, 'kv', axis=1, tiled=True).astype(jnp.float32)  13.1 us
    dot_general x1, matrix products, mixer_block(): down_terms = jnp.dot(activated, w_down, preferred_element_type=jnp.float32)  11.7 us
    dot_general x1, matrix products, mixer_block(): gate_act = jnp.dot(normed, w_gate, preferred_element_type=jnp.float32)  5.9 us
    psum x1, blocking collectives, local(): lax.psum(branch_part.astype(jnp.bfloat16), 'tp').astype(jnp.float32)  3.36 us
  transfers between devices with their start and end apart: 2, of which 2 were waited for; matrix products, arithmetic and copies ran while one was open for 0% of the time, Pallas kernels for 0%

commit v1 on v0

--- a/solution.py
+++ b/solution.py
@@ -1,6 +1,8 @@
 import jax
 import jax.numpy as jnp
 from jax import lax
+from jax.experimental import pallas as pl
+from jax.experimental.pallas import tpu as pltpu
 from jax.sharding import PartitionSpec as P
 
 D = 4096
@@ -47,7 +49,7 @@
     return lax.psum_scatter(down_terms, ("kv", "tp"), scatter_dimension=1, tiled=True)
 
 
-def local(
+def local_plain(
     tokens,
     gain_mix,
     w_query,
@@ -113,7 +115,385 @@
     return (mixed, memory_next, norm_next, stab_next)
 
 
+SUBLANES, LANES = 8, 128
+MESH = pl.DeviceIdType.MESH
+NT = (((1,), (1,)), ((), ()))
+
+
+def fused_kernel(
+    n_kv,
+    n_tp,
+    tok_h, gmix_h, wq_h, wk_h, wv_h, wig_h, wfg_h, big_h, bfg_h, mem_h, nrm_h, stb_h,
+    wo_h, gmlp_h, wg_h, wu_h, wd_h,
+    mixed_h, memn_h, nrmn_h, stbn_h,
+    tok, gmix, wqkv, wig, wfg, big, bfg, mem, nrm, stb, wo, gmlp, wg, wu, wd,
+    memn, nrmn, stbn, mixed,
+    mhi, mlo, scaled_pad,
+    part_send, part_recv, gate_send, gate_recv, cells, hid_send, hid, br_send, br_recv,
+    res, down_send, down_recv,
+    in_sem, out_sem, wg_sem, wu_sem, wd_sem,
+    send_sem, recv_sem,
+):
+    f32, bf16 = jnp.float32, jnp.bfloat16
+    kv, tp, dp = lax.axis_index("kv"), lax.axis_index("tp"), lax.axis_index("dp")
+    rows, width = tok.shape
+    seqs, heads, hd = nrm.shape
+    inner = heads * hd
+    model = width * n_kv
+    own_cols = mixed.shape[1]
+    n_dev = n_kv * n_tp
+
+    def peer(j, s):
+        return lax.rem(kv + j, n_kv), lax.rem(tp + s, n_tp)
+
+    others = [(j, s) for j in range(n_kv) for s in range(n_tp) if (j, s) != (0, 0)]
+    dest_order = sorted(
+        others, key=lambda js: (-min(js[0], n_kv - js[0]), js[0], js[1])
+    ) + [(0, 0)]
+
+    loads = {}
+
+    def load(name, src, dst, sem):
+        loads[name] = pltpu.make_async_copy(src, dst, sem)
+        loads[name].start()
+
+    small = [
+        ("tok", tok_h, tok), ("gmix", gmix_h, gmix), ("wig", wig_h, wig), ("wfg", wfg_h, wfg),
+        ("wq", wq_h, wqkv.at[0]), ("wk", wk_h, wqkv.at[1]), ("wv", wv_h, wqkv.at[2]),
+        ("big", big_h, big), ("bfg", bfg_h, bfg), ("nrm", nrm_h, nrm), ("stb", stb_h, stb),
+        ("mem", mem_h, mem), ("gmlp", gmlp_h, gmlp), ("wo", wo_h, wo),
+    ]
+    for i, (name, src, dst) in enumerate(small):
+        load(name, src, dst, in_sem.at[i])
+    for j in range(n_kv):
+        src = lax.rem(kv + n_kv - j, n_kv)
+        rng = pl.ds(pl.multiple_of(src * width, width), width)
+        load(f"wg{j}", wg_h.at[rng, :], wg.at[j], wg_sem.at[j])
+        load(f"wu{j}", wu_h.at[rng, :], wu.at[j], wu_sem.at[j])
+    for i, (j, s) in enumerate(dest_order):
+        dk, dt = peer(j, s)
+        rng = pl.ds(pl.multiple_of((dk * n_tp + dt) * own_cols, own_cols), own_cols)
+        load(f"wd{i}", wd_h.at[:, rng], wd.at[i], wd_sem.at[i])
+
+    barrier = pltpu.get_barrier_semaphore()
+    for j, s in others:
+        dk, dt = peer(j, s)
+        pl.semaphore_signal(barrier, inc=1, device_id=(dp, dk, dt), device_id_type=MESH)
+
+    count = [0]
+    sends = []
+
+    def send(src, dst, j, s):
+        i = count[0]
+        count[0] += 1
+        dk, dt = peer(j, s)
+        copy = pltpu.make_async_remote_copy(
+            src_ref=src, dst_ref=dst, send_sem=send_sem.at[i], recv_sem=recv_sem.at[i],
+            device_id=(dp, dk, dt), device_id_type=MESH,
+        )
+        copy.start()
+        sends.append(copy)
+        return copy
+
+    loads["tok"].wait()
+    loads["gmix"].wait()
+    tokf = tok[...].astype(f32)
+    scaled = (tokf * gmix[...]).astype(bf16)
+    scaled_pad[...] = jnp.zeros_like(scaled_pad)
+    scaled_pad[0:rows, :] = scaled
+    loads["wig"].wait()
+    loads["wfg"].wait()
+    padded = scaled_pad[...]
+    ig = lax.dot_general(wig[...], padded, NT, preferred_element_type=f32)
+    fg = lax.dot_general(wfg[...], padded, NT, preferred_element_type=f32)
+    squares = jnp.sum(tokf * tokf, axis=1, keepdims=True)
+    lane = lax.broadcasted_iota(jnp.int32, (rows, LANES), 1)
+    row = lax.broadcasted_iota(jnp.int32, (rows, LANES), 0)
+    square_row = jnp.sum(jnp.where(lane == row + 2 * rows, squares, 0.0), axis=0, keepdims=True)
+    gates_own = ig + pltpu.roll(fg, rows, 1) + square_row
+    gate_send[...] = gates_own
+
+    for i, name in enumerate(("wq", "wk", "wv")):
+        loads[name].wait()
+        part = jnp.dot(scaled, wqkv[i], preferred_element_type=f32)
+        for c in range(n_kv):
+            part_send[c, :, i * inner : (i + 1) * inner] = part[c * seqs : (c + 1) * seqs, :]
+
+    pl.semaphore_wait(barrier, n_dev - 1)
+    hops = sorted(range(1, n_kv), key=lambda j: (-min(j, n_kv - j), j))
+    gate_copies, part_copies = {}, {}
+    for j in hops:
+        dk, _ = peer(j, 0)
+        part_copies[j] = send(part_send.at[dk], part_recv.at[j - 1], j, 0)
+        gate_copies[j] = send(gate_send, gate_recv.at[j - 1], j, 0)
+
+    loads["mem"].wait()
+    for b in range(seqs):
+        for h in range(heads):
+            piece = mem[b, h]
+            high = piece.astype(bf16)
+            mhi[b, h * hd : (h + 1) * hd, :] = high
+            mlo[b, h * hd : (h + 1) * hd, :] = (piece - high.astype(f32)).astype(bf16)
+    for name in ("big", "bfg", "nrm", "stb"):
+        loads[name].wait()
+    eye = lax.broadcasted_iota(jnp.int32, (heads, heads), 0) == lax.broadcasted_iota(
+        jnp.int32, (heads, heads), 1
+    )
+
+    def column(row_value):
+        return jnp.sum(jnp.where(eye, row_value, 0.0), axis=1, keepdims=True)
+
+    def as_row(column_value):
+        return jnp.sum(jnp.where(eye, column_value, 0.0), axis=0, keepdims=True)
+
+    bias_i = column(big[...])
+    bias_f = column(bfg[...])
+    block_of = lax.broadcasted_iota(jnp.int32, (heads, inner), 1) // hd
+    head_of = lax.broadcasted_iota(jnp.int32, (heads, inner), 0)
+
+    total = part_send[kv]
+    gates = gates_own
+    for j in hops:
+        gate_copies[j].wait_recv()
+        gates += gate_recv[j - 1]
+    for j in hops:
+        part_copies[j].wait_recv()
+        total += part_recv[j - 1]
+    for b in range(seqs):
+        for i in range(3 * heads):
+            cells[b, i : i + 1, :] = total[b : b + 1, i * hd : (i + 1) * hd]
+    keeps, freshes = [], []
+    for b in range(seqs):
+        at = kv * seqs + b
+
+        def pick(offset):
+            return jnp.sum(jnp.where(lane == at + offset, gates, 0.0), axis=1, keepdims=True)
+
+        scale = lax.rsqrt(pick(2 * rows) / model + epsilon)
+        in_gate = scale * pick(0) + bias_i
+        forget_in = scale * pick(rows) + bias_f
+        log_forget = jnp.minimum(forget_in, 0.0) - jnp.log1p(jnp.exp(-jnp.abs(forget_in)))
+        held = column(stb[b : b + 1, :]) + log_forget
+        stab = jnp.maximum(held, in_gate)
+        keep = jnp.exp(held - stab)
+        fresh = jnp.exp(in_gate - stab)
+        stbn[b : b + 1, :] = as_row(stab)
+        query = (scale * cells[b, 0:heads, :]).astype(bf16)
+        key = (scale * cells[b, heads : 2 * heads, :]).astype(bf16).astype(f32) * hd ** (-0.5)
+        fresh_key = fresh * key
+        cells[b, heads : 2 * heads, :] = fresh_key
+        value = (scale * cells[b, 2 * heads :, :]).astype(bf16).astype(f32)
+        cells[b, 2 * heads :, :] = value
+        queryf = query.astype(f32)
+        norm_next = keep * nrm[b] + fresh_key
+        nrmn[b] = norm_next
+        den = jnp.sum(norm_next * queryf, axis=1, keepdims=True)
+        den = jnp.maximum(jnp.abs(den), jnp.exp(-stab))
+        weight = jnp.sum(fresh_key * queryf, axis=1, keepdims=True)
+        held_part = lax.dot_general(query, mhi[b], NT, preferred_element_type=f32)
+        held_part += lax.dot_general(query, mlo[b], NT, preferred_element_type=f32)
+        value_row = (scale[0:1, :] * total[b : b + 1, 2 * inner :]).astype(bf16).astype(f32)
+        grid = (keep * held_part + weight * value_row) / den
+        hid_send[b : b + 1, :] = jnp.sum(
+            jnp.where(block_of == head_of, grid, 0.0), axis=0, keepdims=True
+        )
+        keeps.append(keep)
+    hid_first = count[0]
+    for j in hops:
+        send(hid_send, hid.at[kv], j, 0)
+    hid[kv] = hid_send[...]
+
+    outs = []
+
+    def store(src, dst):
+        copy = pltpu.make_async_copy(src, dst, out_sem.at[len(outs)])
+        copy.start()
+        outs.append(copy)
+
+    for b in range(seqs):
+        value_t = cells[b, 2 * heads :, :].T
+        for h in range(heads):
+            memn[b, h] = (
+                keeps[b][h : h + 1, :] * mem[b, h]
+                + value_t[:, h : h + 1] * cells[b, heads + h : heads + h + 1, :]
+            )
+
+    loads["wo"].wait()
+    for i, j in enumerate(hops):
+        dk, dt = peer(j, 0)
+        pltpu.make_async_remote_copy(
+            src_ref=hid_send, dst_ref=hid.at[lax.rem(kv + n_kv - j, n_kv)],
+            send_sem=send_sem.at[hid_first + i], recv_sem=recv_sem.at[hid_first + i],
+            device_id=(dp, dk, dt), device_id_type=MESH,
+        ).wait_recv()
+    hidden = jnp.concatenate([hid[c] for c in range(n_kv)], axis=0).astype(bf16)
+    branch = jnp.dot(hidden, wo[...], preferred_element_type=f32).astype(bf16)
+    br_send[...] = branch
+    partner_copies = [send(br_send, br_recv.at[s - 1], 0, s) for s in range(1, n_tp)]
+    store(memn, memn_h)
+    store(nrmn, nrmn_h)
+    store(stbn, stbn_h)
+    for copy in partner_copies:
+        copy.wait_recv()
+    branch_sum = branch.astype(f32)
+    for s in range(1, n_tp):
+        branch_sum += br_recv[s - 1].astype(f32)
+    res[0] = (tokf + branch_sum).astype(bf16)
+    res_copies = {j: send(res.at[0], res.at[j], j, 0) for j in hops}
+
+    loads["gmlp"].wait()
+    near = [0] + sorted(range(1, n_kv), key=lambda j: (min(j, n_kv - j), j))
+    sums = jnp.zeros((rows, 1), f32)
+    gate_acc = jnp.zeros((rows, wg.shape[2]), f32)
+    up_acc = jnp.zeros((rows, wg.shape[2]), f32)
+    for j in near:
+        loads[f"wg{j}"].wait()
+        loads[f"wu{j}"].wait()
+        if j:
+            res_copies[j].wait_recv()
+        chunk = res[j].astype(f32)
+        src_kv = lax.rem(kv + n_kv - j, n_kv)
+        sums += jnp.sum(chunk * chunk, axis=1, keepdims=True)
+        lhs = (chunk * gmlp[src_kv]).astype(bf16)
+        gate_acc += jnp.dot(lhs, wg[j], preferred_element_type=f32)
+        up_acc += jnp.dot(lhs, wu[j], preferred_element_type=f32)
+    scale = lax.rsqrt(sums / model + epsilon)
+    gate = scale * gate_acc
+    activated = (gate * jax.nn.sigmoid(gate) * (scale * up_acc)).astype(bf16)
+
+    down_copies = []
+    own = None
+    for i, (j, s) in enumerate(dest_order):
+        loads[f"wd{i}"].wait()
+        block = jnp.dot(activated, wd[i], preferred_element_type=f32)
+        if (j, s) == (0, 0):
+            own = block
+        else:
+            down_send[i] = block
+            down_copies.append(send(down_send.at[i], down_recv.at[i], j, s))
+    mine = pl.ds(pl.multiple_of(tp * own_cols, own_cols), own_cols)
+    for i, copy in enumerate(down_copies):
+        copy.wait_recv()
+        own += down_recv[i]
+    mixed[...] = (res[0, :, mine].astype(f32) + own).astype(bf16)
+    store(mixed, mixed_h)
+    for copy in sends:
+        copy.wait_send()
+    for copy in outs:
+        copy.wait()
+
+
+def fused(
+    n_kv, n_tp,
+    tokens, gain_mix, w_query, w_key, w_value, w_igate, w_fgate, bias_igate, bias_fgate,
+    memory, normalizer, stabilizer, w_output, gain_mlp, w_gate, w_up, w_down,
+):
+    f32, bf16 = jnp.float32, jnp.bfloat16
+    rows, width = tokens.shape
+    seqs, heads, hd = normalizer.shape
+    inner = heads * hd
+    units = w_gate.shape[1]
+    n_dev = n_kv * n_tp
+    own_cols = width // n_tp
+    copies = 4 * (n_kv - 1) + (n_tp - 1) + (n_dev - 1)
+    anyspec = pl.BlockSpec(memory_space=pl.ANY)
+    dma = pltpu.SemaphoreType.DMA
+    out_shape = (
+        jax.ShapeDtypeStruct((rows, own_cols), bf16),
+        jax.ShapeDtypeStruct(memory.shape, f32),
+        jax.ShapeDtypeStruct(normalizer.shape, f32),
+        jax.ShapeDtypeStruct(stabilizer.shape, f32),
+    )
+    scratch = [
+        pltpu.VMEM((rows, width), bf16),
+        pltpu.VMEM((1, width), f32),
+        pltpu.VMEM((3, width, inner), bf16),
+        pltpu.VMEM((heads, width), bf16),
+        pltpu.VMEM((heads, width), bf16),
+        pltpu.VMEM((1, heads), f32),
+        pltpu.VMEM((1, heads), f32),
+        pltpu.VMEM(memory.shape, f32),
+        pltpu.VMEM(normalizer.shape, f32),
+        pltpu.VMEM(stabilizer.shape, f32),
+        pltpu.VMEM((inner, width), bf16),
+        pltpu.VMEM((n_kv, 1, width), f32),
+        pltpu.VMEM((n_kv, width, units), bf16),
+        pltpu.VMEM((n_kv, width, units), bf16),
+        pltpu.VMEM((n_dev, units, own_cols), bf16),
+        pltpu.VMEM(memory.shape, f32),
+        pltpu.VMEM(normalizer.shape, f32),
+        pltpu.VMEM(stabilizer.shape, f32),
+        pltpu.VMEM((rows, own_cols), bf16),
+        pltpu.VMEM((seqs, inner, hd), bf16),
+        pltpu.VMEM((seqs, inner, hd), bf16),
+        pltpu.VMEM((LANES, width), bf16),
+        pltpu.VMEM((n_kv, seqs, 3 * inner), f32),
+        pltpu.VMEM((n_kv - 1, seqs, 3 * inner), f32),
+        pltpu.VMEM((heads, LANES), f32),
+        pltpu.VMEM((n_kv - 1, heads, LANES), f32),
+        pltpu.VMEM((seqs, 3 * heads, hd), f32),
+        pltpu.VMEM((seqs, inner), f32),
+        pltpu.VMEM((n_kv, seqs, inner), f32),
+        pltpu.VMEM((rows, width), bf16),
+        pltpu.VMEM((n_tp - 1, rows, width), bf16),
+        pltpu.VMEM((n_kv, rows, width), bf16),
+        pltpu.VMEM((n_dev, rows, own_cols), f32),
+        pltpu.VMEM((n_dev - 1, rows, own_cols), f32),
+        dma((14,)),
+        dma((4,)),
+        dma((n_kv,)),
+        dma((n_kv,)),
+        dma((n_dev,)),
+        dma((copies,)),
+        dma((copies,)),
+    ]
+
+    def body(*refs):
+        fused_kernel(n_kv, n_tp, *refs)
+
+    return pl.pallas_call(
+        body,
+        out_shape=out_shape,
+        in_specs=[anyspec] * 17,
+        out_specs=(anyspec,) * 4,
+        scratch_shapes=scratch,
+        compiler_params=pltpu.CompilerParams(
+            collective_id=0, has_side_effects=True, vmem_limit_bytes=62 * 2**20
+        ),
+    )(
+        tokens, gain_mix.reshape(1, width), w_query, w_key, w_value, w_igate.T, w_fgate.T,
+        bias_igate.reshape(1, heads), bias_fgate.reshape(1, heads), memory, normalizer, stabilizer,
+        w_output, gain_mlp.reshape(n_kv, 1, width), w_gate, w_up, w_down,
+    )
+
+
+def fits(n_kv, n_tp, tokens, normalizer, w_gate):
+    rows, width = tokens.shape
+    seqs, heads, hd = normalizer.shape
+    units = w_gate.shape[1]
+    weights = 2 * width * (4 * heads * hd + 3 * units * n_kv) + 16 * seqs * heads * hd * hd
+    return (
+        n_kv > 1
+        and n_tp > 1
+        and rows == SUBLANES
+        and heads == SUBLANES
+        and hd == LANES
+        and seqs * n_kv == rows
+        and width % (n_tp * LANES) == 0
+        and units % LANES == 0
+        and weights < 58 * 2**20
+    )
+
+
 def solution(mesh):
+    n_kv, n_tp = mesh.shape["kv"], mesh.shape["tp"]
+
+    def local(*args):
+        tokens, normalizer, w_gate = args[0], args[10], args[14]
+        if fits(n_kv, n_tp, tokens, normalizer, w_gate):
+            return fused(n_kv, n_tp, *args)
+        return local_plain(*args)
+
     placed = (
         P("dp", "kv"),
         P("kv"),

time: 147 us -> 34.2 us (0.23)
  waiting for transfers between devices: 67.4 us -> 0 us
  blocking collectives: 29.8 us -> 0 us
  Pallas kernels: 0 us -> 28.5 us
  matrix products: 25.7 us -> 0 us
  between operations: 14.9 us -> 0.66 us
  other arithmetic: 7.7 us -> 0 us
  local copies, waits for them, and re-layouts: 0.75 us -> 4.76 us
    unnamed x3 -> x0, waiting for transfers between devices: 36.6 us -> none
    reduce_scatter x1 -> x0, waiting for transfers between devices: 30.8 us -> none  [mixer_block(): lax.psum_scatter(down_terms, ('kv', 'tp'), scatter_dimension=1, tiled=True)]
    pallas_call x0 -> x1, Pallas kernels: none -> 28.5 us  [fused(): pl.pallas_call(body, out_shape=out_shape, in_specs=[anyspec] * 17, out_sp...]
    all_gather x2 -> x0, blocking collectives: 26.5 us -> none  [the longest x1 13.3 us: local(): lax.all_gather(hidden, 'kv', axis=0, tiled=True)]
    dot_general x9 -> x0, matrix products: 25.7 us -> none  [the longest x1 11.7 us: mixer_block(): down_terms = jnp.dot(activated, w_down, preferred_element_type=jnp.float32)]
    unnamed x33 -> x8, local copies, waits for them, and re-layouts: 0.74 us -> 4.76 us
    psum x1 -> x0, blocking collectives: 3.36 us -> none  [local(): lax.psum(branch_part.astype(jnp.bfloat16), 'tp').astype(jnp.float32)]
    convert_element_type x4 -> x0, other arithmetic: 2.28 us -> none  [the longest x1 1.32 us: local(): (residual_own.astype(jnp.float32) + mixed_terms).astype(jnp.bfloat16)]
  transfers between devices with their start and end apart: 2 -> 0, of which waited for: 2 -> 0; matrix products, arithmetic and copies ran while one was open for 0% -> 0% of each run, Pallas kernels for 0% -> 0%
where the time goes in v1:
time: 34.2 us; the launch traced here: 33.9 us
  Pallas kernels  28.5 us (83%)
  local copies, waits for them, and re-layouts  4.76 us (14%)
  between operations  0.66 us (2%)
    pallas_call x1, Pallas kernels, fused(): pl.pallas_call(body, out_shape=out_shape, in_specs=[anyspec] * 17, out_sp...  28.5 us
    unnamed x8, local copies, waits for them, and re-layouts  4.76 us

profile of v1, /device:TPU:0, one launch (start us, length us, event | category | flops | bytes accessed | tf_op | source)
XLA Modules:
  0.0 33.9 jit_solution(3320132573957475528)
XLA Ops:
  0.6 28.5 %shard_map.192 = (bf16[8,512]{1,0:T(8,128)(2,1)}, f32[2,8,128,128]{3,2,1,0:T(8,128)}, f32[2,8,128]{2,1,0:T(8,128)}, f32[2,8]{1,0:T(2,128)}) custom-call(bf16[8,1024]{1,0:T(8,128)(2,1)} %refs_0_.1, f32[1,1024]{1,0:T(1,128)} %bitcast.9, bf16[1024,1024]{1,0:T(8,128)(2,1)} %refs_2_.1, bf16[1024,1024]{1,0:T(8,128)(2,1)} %refs_3_.1, bf16[1024,1024]{1,0:T(8,128)(2,1)} %refs_4_.1, ...), custom_call_target="tpu_custom_call" | custom-call | tf_op jit(solution)/shard_map/pallas_call | solution.py:454
  29.2 0.0 copy-start
  29.2 0.0 copy-start.1
  29.2 1.3 %copy.25 = bf16[8,512]{1,0:T(8,128)(2,1)} copy(bf16[8,512]{1,0:T(8,128)(2,1)} %get-tuple-element.8) | data formatting | bytes 16384
  30.5 2.3 %copy.26 = f32[2,8,128,128]{3,2,1,0:T(8,128)} copy(f32[2,8,128,128]{3,2,1,0:T(8,128)} %get-tuple-element.9) | data formatting | bytes 2097152
  32.8 0.0 copy-done
  32.8 0.6 %copy.27 = f32[2,8,128]{2,1,0:T(8,128)} copy(f32[2,8,128]{2,1,0:T(8,128)S(1)} %copy-done) | data formatting | bytes 16384
  33.4 0.0 copy-done.1
  33.4 0.6 %copy.28 = f32[2,8]{1,0:T(2,128)} copy(f32[2,8]{1,0:T(2,128)S(1)} %copy-done.1) | data formatting | bytes 128
Async XLA Ops:
  29.2 3.6 %copy-start = (f32[2,8,128]{2,1,0:T(8,128)S(1)}, f32[2,8,128]{2,1,0:T(8,128)}, u32[]{:S(2)}) copy-start(f32[2,8,128]{2,1,0:T(8,128)} %get-tuple-element.10) | copy-start | bytes 24580
  29.2 4.2 %copy-start.1 = (f32[2,8]{1,0:T(2,128)S(1)}, f32[2,8]{1,0:T(2,128)}, u32[]{:S(2)}) copy-start(f32[2,8]{1,0:T(2,128)} %get-tuple-element.11) | copy-start | bytes 196
